TPU v7x, 32 devices: a whole 2x2x4 slice. The times are simulated.
32 devices in a mesh: fs: 8 (over z, x), tp: 4 (over y, core).
Axes of the slice: x: 2, y: 2, z: 4, core: 2. Of those that a mesh axis runs over, the one named last changes fastest.
Arguments:
- tokens: bfloat16 [4096, 2048], P(('fs', 'tp')), may hold values from -6 to 6
- gate_weight: bfloat16 [5632, 2048], P('tp', 'fs'), may hold values from -0.125 to 0.125
- up_weight: bfloat16 [5632, 2048], P('tp', 'fs'), may hold values from -0.125 to 0.125
- down_weight: bfloat16 [5632, 2048], P('tp', 'fs'), may hold values from -0.078125 to 0.078125
- out_grad: bfloat16 [4096, 2048], P(('fs', 'tp')), may hold values from -6 to 6
Outputs:
- grad_tokens: bfloat16 [4096, 2048], P(('fs', 'tp'))
- grad_gate: float32 [5632, 2048], P('tp', 'fs')
- grad_up: float32 [5632, 2048], P('tp', 'fs')
- grad_down: float32 [5632, 2048], P('tp', 'fs')
- gate_rows: float32 [5632], P('tp')
- up_rows: float32 [5632], P('tp')
- down_rows: float32 [5632], P('tp')
All inputs are finite; a program needn't handle non-finite values.
Results may differ from a plain program's by a relative error of at most 0.014.
Values may be sent and summed in bfloat16 or wider, within the bound.
A program may use at most 128 MiB of HBM per device.

v0:
```python
import math
import jax
import jax.numpy as jnp
from jax import lax
from jax.sharding import PartitionSpec as P


def body(tokens, gate_weight, up_weight, down_weight, out_grad):
    inputs, cotangent = (
        lax.all_gather(tokens, "tp", axis=0, tiled=True),
        lax.all_gather(out_grad, "tp", axis=0, tiled=True),
    )
    w_gate, w_up, w_down = (
        lax.all_gather(gate_weight, "fs", axis=1, tiled=True),
        lax.all_gather(up_weight, "fs", axis=1, tiled=True),
        lax.all_gather(down_weight, "fs", axis=1, tiled=True),
    )
    inner = (((1,), (1,)), ((), ()))
    gate = lax.dot_general(inputs, w_gate, inner, preferred_element_type=jnp.float32)
    up = lax.dot_general(inputs, w_up, inner, preferred_element_type=jnp.float32)
    dhidden = lax.dot_general(cotangent, w_down, inner, preferred_element_type=jnp.float32)
    sig = jax.nn.sigmoid(gate)
    silu = gate * sig
    act = (silu * up).astype(jnp.bfloat16)
    dgate = (dhidden * up * sig * (1.0 + gate * (1.0 - sig))).astype(jnp.bfloat16)
    dup = (dhidden * silu).astype(jnp.bfloat16)
    term = jnp.dot(dgate, w_gate, preferred_element_type=jnp.float32)
    grad_tokens = lax.psum_scatter(
        (term + jnp.dot(dup, w_up, preferred_element_type=jnp.float32)).astype(jnp.bfloat16),
        "tp",
        scatter_dimension=0,
        tiled=True,
    )
    factor = 1.0 / math.sqrt(inputs.shape[0] * lax.axis_size("fs"))
    outer = (((0,), (0,)), ((), ()))
    width = gate_weight.shape[1] * lax.axis_size("fs")
    part_gate = lax.dot_general(dgate, inputs, outer, preferred_element_type=jnp.float32) * factor
    part_up = lax.dot_general(dup, inputs, outer, preferred_element_type=jnp.float32) * factor
    part_down = lax.dot_general(act, cotangent, outer, preferred_element_type=jnp.float32) * factor
    grad_gate, grad_up, grad_down = (
        lax.psum_scatter(
            part_gate.astype(jnp.bfloat16), "fs", scatter_dimension=1, tiled=True
        ).astype(jnp.float32),
        lax.psum_scatter(
            part_up.astype(jnp.bfloat16), "fs", scatter_dimension=1, tiled=True
        ).astype(jnp.float32),
        lax.psum_scatter(
            part_down.astype(jnp.bfloat16), "fs", scatter_dimension=1, tiled=True
        ).astype(jnp.float32),
    )
    sums = lax.psum(
        (
            jnp.sum(grad_gate * grad_gate, axis=1),
            jnp.sum(grad_up * grad_up, axis=1),
            jnp.sum(grad_down * grad_down, axis=1),
        ),
        "fs",
    )
    gate_rows, up_rows, down_rows = (sums[0] / width, sums[1] / width, sums[2] / width)
    return (grad_tokens, grad_gate, grad_up, grad_down, gate_rows, up_rows, down_rows)


def solution(mesh):
    return jax.shard_map(
        body,
        mesh=mesh,
        in_specs=(
            P(("fs", "tp"), None),
            P("tp", "fs"),
            P("tp", "fs"),
            P("tp", "fs"),
            P(("fs", "tp"), None),
        ),
        out_specs=(
            P(("fs", "tp"), None),
            P("tp", "fs"),
            P("tp", "fs"),
            P("tp", "fs"),
            P("tp"),
            P("tp"),
            P("tp"),
        ),
        check_vma=False,
    )
```

profile of v0, /device:TPU:0, one launch (start us, length us, event | category | flops | bytes accessed | tf_op | source)
XLA Modules:
  0.0 727.2 jit_solution(359217630501200977)
XLA Ops:
  7.2 0.7 all-gather.10.cloned.1.call-update
  7.9 0.7 all-gather.12.cloned.1.call-update
  8.7 0.7 all-gather.14.cloned.1.call-update
  10.6 24.3 %all-gather.10.cloned.1.call-done = bf16[512,2048]{1,0:T(8,128)(2,1)} async-done(((bf16[128,2048]{1,0:T(8,128)(2,1)}), bf16[512,2048]{1,0:T(8,128)(2,1)}) %all-gather.10.cloned.1.call-update) | async-done | bytes 2097168 | tf_op jit(solution)/shard_map/all_gather | solution.py:10
  34.9 95.2 %all-gather.12.cloned.1.call-done = bf16[1408,2048]{1,0:T(8,128)(2,1)} async-done(((bf16[1408,256]{1,0:T(8,128)(2,1)}), bf16[1408,2048]{1,0:T(8,128)(2,1)}) %all-gather.12.cloned.1.call-update) | async-done | bytes 5767184 | tf_op jit(solution)/shard_map/all_gather | solution.py:15
  130.1 8.3 %fusion.3 = f32[512,1408]{1,0:T(8,128)} fusion(bf16[512,2048]{1,0:T(8,128)(2,1)} %all-gather.10.cloned.1.call-done, bf16[1408,2048]{1,0:T(8,128)(2,1)} %all-gather.12.cloned.1.call-done), kind=kOutput, calls=%fused_computation.16 | convolution fusion | flops 2952790016 | bytes 10747904 | tf_op jit(solution)/shard_map/dot_general | solution.py:20
  138.4 85.1 %all-gather.14.cloned.1.call-done = bf16[1408,2048]{1,0:T(8,128)(2,1)} async-done(((bf16[1408,256]{1,0:T(8,128)(2,1)}), bf16[1408,2048]{1,0:T(8,128)(2,1)}) %all-gather.14.cloned.1.call-update) | async-done | bytes 5767184 | tf_op jit(solution)/shard_map/all_gather | solution.py:14
  223.5 7.6 %fusion.4 = f32[512,1408]{1,0:T(8,128)} fusion(bf16[512,2048]{1,0:T(8,128)(2,1)S(1)} %copy-done, bf16[1408,2048]{1,0:T(8,128)(2,1)} %all-gather.14.cloned.1.call-done), kind=kOutput, calls=%fused_computation.17 | convolution fusion | flops 2952790016 | bytes 10747904 | tf_op jit(solution)/shard_map/dot_general | solution.py:19
  231.1 14.6 %all-gather.6.cloned.1.call-done = bf16[512,2048]{1,0:T(8,128)(2,1)} async-done(((bf16[128,2048]{1,0:T(8,128)(2,1)}), bf16[512,2048]{1,0:T(8,128)(2,1)}) %all-gather.6.cloned.1.call-update) | async-done | bytes 2097168 | tf_op jit(solution)/shard_map/all_gather | solution.py:11
  245.7 9.1 %multiply_convert_fusion = bf16[1408,2048]{1,0:T(8,128)(2,1)} fusion(bf16[512,2048]{1,0:T(8,128)(2,1)} %all-gather.6.cloned.1.call-done, f32[512,1408]{1,0:T(8,128)} %fusion.3, f32[512,1408]{1,0:T(8,128)} %fusion.4), kind=kOutput, calls=%fused_computation | convolution fusion | flops 2962882560 | bytes 13631488 | tf_op jit(solution)/shard_map/dot_general | solution.py:39
  255.0 85.7 %all-gather.8.cloned.1.call-done = bf16[1408,2048]{1,0:T(8,128)(2,1)} async-done(((bf16[1408,256]{1,0:T(8,128)(2,1)}), bf16[1408,2048]{1,0:T(8,128)(2,1)}) %all-gather.8.cloned.1.call-update) | async-done | bytes 5767184 | tf_op jit(solution)/shard_map/all_gather | solution.py:16
  340.7 10.2 %multiply_convert_fusion.4 = (bf16[512,1408]{1,0:T(8,128)(2,1)S(1)}, bf16[512,1408]{1,0:T(8,128)(2,1)}) fusion(f32[512,1408]{1,0:T(8,128)} %fusion.4, f32[512,1408]{1,0:T(8,128)} %fusion.3, bf16[512,2048]{1,0:T(8,128)(2,1)} %all-gather.6.cloned.1.call-done, bf16[1408,2048]{1,0:T(8,128)(2,1)} %all-gather.8.cloned.1.call-done), kind=kOutput, calls=%fused_computation.5 | convolution fusion | flops 2962161664 | bytes 16515072 | tf_op jit(solution)/shard_map/dot_general | solution.py:21
  350.9 5.0 multiply_convert_fusion.1
  355.9 6.5 multiply_convert_fusion.2
  362.5 1.3 copy-done.1
  363.8 5.4 fusion.5
  369.2 7.4 %add_convert_fusion = bf16[512,2048]{1,0:T(8,128)(2,1)} fusion(f32[512,2048]{1,0:T(8,128)S(1)} %fusion.5, bf16[512,1408]{1,0:T(8,128)(2,1)S(1)} %get-tuple-element.16, bf16[1408,2048]{1,0:T(8,128)(2,1)} %all-gather.12.cloned.1.call-done), kind=kOutput, calls=%fused_computation.3 | convolution fusion | flops 2954887168 | bytes 13500416 | tf_op jit(solution)/shard_map/dot_general | solution.py:29
  376.6 76.8 %reduce-scatter.11.cloned.1.call-done = bf16[1408,256]{1,0:T(8,128)(2,1)} async-done(((bf16[1408,2048]{1,0:T(8,128)(2,1)}), bf16[1408,256]{1,0:T(8,128)(2,1)}) %reduce-scatter.11.cloned.1.call-update) | async-done | bytes 720912 | tf_op jit(solution)/shard_map/reduce_scatter | solution.py:47
  453.5 2.3 multiply_reduce_fusion
  455.8 111.8 %reduce-scatter.9.cloned.1.call-done = bf16[1408,256]{1,0:T(8,128)(2,1)} async-done(((bf16[1408,2048]{1,0:T(8,128)(2,1)}), bf16[1408,256]{1,0:T(8,128)(2,1)}) %reduce-scatter.9.cloned.1.call-update) | async-done | bytes 720912 | tf_op jit(solution)/shard_map/reduce_scatter | solution.py:44
  567.6 2.3 multiply_reduce_fusion.1
  569.9 111.8 %reduce-scatter.7.cloned.1.call-done = bf16[1408,256]{1,0:T(8,128)(2,1)} async-done(((bf16[1408,2048]{1,0:T(8,128)(2,1)}), bf16[1408,256]{1,0:T(8,128)(2,1)}) %reduce-scatter.7.cloned.1.call-update) | async-done | bytes 720912 | tf_op jit(solution)/shard_map/reduce_scatter | solution.py:41
  681.7 2.3 multiply_reduce_fusion.2
  684.0 35.5 %all-reduce = (f32[1408]{0:T(1024)S(1)}, f32[1408]{0:T(1024)S(1)}, f32[1408]{0:T(1024)S(1)}) all-reduce(f32[1408]{0:T(1024)S(1)} %get-tuple-element.14, f32[1408]{0:T(1024)S(1)} %get-tuple-element.12, f32[1408]{0:T(1024)S(1)} %get-tuple-element.10), channel_id=1, replica_groups=mesh['fs'=8,'tp'=4] {'fs'}, use_global_device_ids=true, to_apply=%region_5.0 | all-reduce | flops 4224 | bytes 33792 | tf_op jit(solution)/shard_map/psum | solution.py:51
  (21 shorter events, 2.9 us)
Async XLA Ops:
  7.2 27.7 %all-gather.10.cloned.1.call-start = ((), (), s32[]{:S(2)}) async-start(), calls=%async_computation.6 | async-start | bytes 2621440 | tf_op jit(solution)/shard_map/all_gather | solution.py:10
  7.9 122.2 %all-gather.12.cloned.1.call-start = ((), (), s32[]{:S(2)}) async-start(), calls=%async_computation.7 | async-start | bytes 6488064 | tf_op jit(solution)/shard_map/all_gather | solution.py:15
  8.6 214.8 %all-gather.14.cloned.1.call-start = ((), (), s32[]{:S(2)}) async-start(), calls=%async_computation.8 | async-start | bytes 6488064 | tf_op jit(solution)/shard_map/all_gather | solution.py:14
  9.4 236.3 %all-gather.6.cloned.1.call-start = ((), (), s32[]{:S(2)}) async-start(), calls=%async_computation.4 | async-start | bytes 2621440 | tf_op jit(solution)/shard_map/all_gather | solution.py:11
  10.0 330.7 %all-gather.8.cloned.1.call-start = ((), (), s32[]{:S(2)}) async-start(), calls=%async_computation.5 | async-start | bytes 6488064 | tf_op jit(solution)/shard_map/all_gather | solution.py:16
  10.5 442.9 %reduce-scatter.11.cloned.1.call-start = ((), (), s32[]{:S(2)}) async-start(), calls=%async_computation.12 | async-start | bytes 6488064 | tf_op jit(solution)/shard_map/reduce_scatter | solution.py:47
  34.9 188.6 %copy-start = (bf16[512,2048]{1,0:T(8,128)(2,1)S(1)}, bf16[512,2048]{1,0:T(8,128)(2,1)}, u32[]{:S(2)}) copy-start(bf16[512,2048]{1,0:T(8,128)(2,1)} %all-gather.10.cloned.1.call-done) | copy-start | bytes 6291460
  254.7 312.8 %reduce-scatter.9.cloned.1.call-start = ((), (), s32[]{:S(2)}) async-start(), calls=%async_computation.11 | async-start | bytes 6488064 | tf_op jit(solution)/shard_map/reduce_scatter | solution.py:44
  355.9 325.8 %reduce-scatter.7.cloned.1.call-start = ((), (), s32[]{:S(2)}) async-start(), calls=%async_computation.10 | async-start | bytes 6488064 | tf_op jit(solution)/shard_map/reduce_scatter | solution.py:41
  362.4 1.4 copy-start.1
  362.4 358.3 %reduce-scatter.5.cloned.1.call-start = ((), (), s32[]{:S(2)}) async-start(), calls=%async_computation.9 | async-start | bytes 2621440 | tf_op jit(solution)/shard_map/reduce_scatter | solution.py:28
Sparse Core Ops, SparseCore 0:
  9.5 25.2 all-gather.9
  36.9 93.1 all-gather.11
  132.1 91.3 all-gather.13
  224.9 20.7 all-gather.5
  247.5 93.1 all-gather.7
  344.2 109.1 reduce-scatter.10
  457.1 110.3 reduce-scatter.8
  571.2 110.3 reduce-scatter.6
  684.8 30.5 reduce-scatter.4
where the time goes:
time: 728 us; the launch traced here: 727 us
  waiting for transfers between devices  608 us (84%)
  matrix products  59.5 us (8%)
  blocking collectives  35.5 us (5%)
  between operations  13.9 us (2%)
  other arithmetic  8.24 us (1%)
    reduce_scatter x1, waiting for transfers between devices, body(): lax.psum_scatter(part_up.astype(jnp.bfloat16), 'fs', scatter_dimension=1,...  112 us
    reduce_scatter x1, waiting for transfers between devices, body(): lax.psum_scatter(part_gate.astype(jnp.bfloat16), 'fs', scatter_dimension=...  112 us
    all_gather x1, waiting for transfers between devices, body(): lax.all_gather(up_weight, 'fs', axis=1, tiled=True)  95.2 us
    all_gather x1, waiting for transfers between devices, body(): lax.all_gather(down_weight, 'fs', axis=1, tiled=True)  85.7 us
    all_gather x1, waiting for transfers between devices, body(): lax.all_gather(gate_weight, 'fs', axis=1, tiled=True)  85.1 us
    reduce_scatter x1, waiting for transfers between devices, body(): lax.psum_scatter(part_down.astype(jnp.bfloat16), 'fs', scatter_dimension=...  76.8 us
    psum x1, blocking collectives, body(): lax.psum((jnp.sum(grad_gate * grad_gate, axis=1), jnp.sum(grad_up * grad_...  35.5 us
    all_gather x1, waiting for transfers between devices, body(): lax.all_gather(tokens, 'tp', axis=0, tiled=True)  24.3 us
  transfers between devices with their start and end apart: 9, of which 8 were waited for; matrix products, arithmetic and copies ran while one was open for 9% of the time, Pallas kernels for 0%

commit v1 on v0

--- a/solution.py
+++ b/solution.py
@@ -3,6 +3,18 @@
 import jax.numpy as jnp
 from jax import lax
 from jax.sharding import PartitionSpec as P
+
+
+def doubled_up(array, axis, dim):
+    ways, here, step = (lax.axis_size(axis), lax.axis_index(axis), array.shape[dim])
+    line, have = (array, 1)
+    while have < ways:
+        line = jnp.concatenate(
+            [line, lax.ppermute(line, axis, [(d, (d - have) % ways) for d in range(ways)])],
+            axis=dim,
+        )
+        have = 2 * have
+    return jnp.roll(line, here * step, axis=dim)
 
 
 def body(tokens, gate_weight, up_weight, down_weight, out_grad):
@@ -13,7 +25,7 @@
     w_gate, w_up, w_down = (
         lax.all_gather(gate_weight, "fs", axis=1, tiled=True),
         lax.all_gather(up_weight, "fs", axis=1, tiled=True),
-        lax.all_gather(down_weight, "fs", axis=1, tiled=True),
+        doubled_up(down_weight, "fs", 1),
     )
     inner = (((1,), (1,)), ((), ()))
     gate = lax.dot_general(inputs, w_gate, inner, preferred_element_type=jnp.float32)

time: 728 us -> 760 us (1.044)
  local copies, waits for them, and re-layouts: 1.29 us -> 17.2 us
  waiting for transfers between devices: 608 us -> 616 us
    ppermute x0 -> x3, waiting for transfers between devices: none -> 259 us  [doubled_up(): lax.ppermute(line, axis, [(d, (d - have) % ways) for d in range(ways)])]
    all_gather x1 -> x0, waiting for transfers between devices: 85.7 us -> none  [body(): lax.all_gather(down_weight, 'fs', axis=1, tiled=True)]
    all_gather x1, waiting for transfers between devices: 85.1 us -> 0.01 us  [body(): lax.all_gather(gate_weight, 'fs', axis=1, tiled=True)]
    all_gather x1, waiting for transfers between devices: 95.2 us -> 36.5 us  [body(): lax.all_gather(up_weight, 'fs', axis=1, tiled=True)]
    reduce_scatter x1, waiting for transfers between devices: 76.8 us -> 112 us  [body(): lax.psum_scatter(part_down.astype(jnp.bfloat16), 'fs', scatter_dimension=...]
    reduce_scatter x1, waiting for transfers between devices: 112 us -> 80.6 us  [body(): lax.psum_scatter(part_up.astype(jnp.bfloat16), 'fs', scatter_dimension=1,...]
    all_gather x1, waiting for transfers between devices: 24.3 us -> 0.01 us  [body(): lax.all_gather(tokens, 'tp', axis=0, tiled=True)]
    unnamed x4 -> x15, local copies, waits for them, and re-layouts: 1.29 us -> 13.4 us
  transfers between devices with their start and end apart: 9 -> 11, of which waited for: 8 -> 8; matrix products, arithmetic and copies ran while one was open for 9% -> 9% of each run, Pallas kernels for 0% -> 0%
where the time goes in v1:
time: 760 us
  waiting for transfers between devices  616 us (81%)
  matrix products  57.9 us (8%)
  blocking collectives  35.5 us (5%)
  local copies, waits for them, and re-layouts  17.2 us (2%)
  between operations  14.2 us (2%)
  other arithmetic  11.5 us (2%)
  starting transfers between devices  7.86 us (1%)
    ppermute x3, waiting for transfers between devices, doubled_up(): lax.ppermute(line, axis, [(d, (d - have) % ways) for d in range(ways)])  259 us
    reduce_scatter x1, waiting for transfers between devices, body(): lax.psum_scatter(part_down.astype(jnp.bfloat16), 'fs', scatter_dimension=...  112 us
    reduce_scatter x1, waiting for transfers between devices, body(): lax.psum_scatter(part_gate.astype(jnp.bfloat16), 'fs', scatter_dimension=...  112 us
    reduce_scatter x1, waiting for transfers between devices, body(): lax.psum_scatter(part_up.astype(jnp.bfloat16), 'fs', scatter_dimension=1,...  80.6 us
    all_gather x1, waiting for transfers between devices, body(): lax.all_gather(up_weight, 'fs', axis=1, tiled=True)  36.5 us
    psum x1, blocking collectives, body(): lax.psum((jnp.sum(grad_gate * grad_gate, axis=1), jnp.sum(grad_up * grad_...  35.5 us
  transfers between devices with their start and end apart: 11, of which 8 were waited for; matrix products, arithmetic and copies ran while one was open for 9% of the time, Pallas kernels for 0%

profile of v1, /device:TPU:0, one launch (start us, length us, event | category | flops | bytes accessed | tf_op | source)
XLA Modules:
  0.0 759.9 jit_solution(9355302498072230193)
XLA Ops:
  9.4 6.1 collective-permute-start
  15.5 15.7 %collective-permute-done = bf16[1408,256]{1,0:T(8,128)(2,1)S(1)} collective-permute-done((bf16[1408,256]{1,0:T(8,128)(2,1)}, bf16[1408,256]{1,0:T(8,128)(2,1)S(1)}, u32[]{:S(2)}, u32[]{:S(2)}) %collective-permute-start) | collective-permute-done | bytes 720928 | tf_op jit(solution)/shard_map/ppermute | solution.py:13
  33.9 52.2 %collective-permute-done.1 = bf16[1408,512]{1,0:T(8,128)(2,1)S(1)} collective-permute-done((bf16[1408,512]{1,0:T(8,128)(2,1)S(1)}, bf16[1408,512]{1,0:T(8,128)(2,1)S(1)}, u32[]{:S(2)}, u32[]{:S(2)}) %collective-permute-start.1) | collective-permute-done | bytes 1441824 | tf_op jit(solution)/shard_map/ppermute | solution.py:13
  86.2 2.0 pad_maximum_fusion
  91.4 190.6 %collective-permute-done.2 = bf16[1408,1024]{1,0:T(8,128)(2,1)} collective-permute-done((bf16[1408,1024]{1,0:T(8,128)(2,1)}, bf16[1408,1024]{1,0:T(8,128)(2,1)}, u32[]{:S(2)}, u32[]{:S(2)}) %collective-permute-start.2) | collective-permute-done | bytes 2883616 | tf_op jit(solution)/shard_map/ppermute | solution.py:13
  282.0 3.7 constant_dynamic-update-slice_fusion.4
  289.0 3.7 constant_dynamic-update-slice_fusion
  292.7 8.2 %fusion.10 = f32[512,1408]{0,1:T(8,128)} fusion(bf16[512,2048]{1,0:T(8,128)(2,1)} %all-gather.7.cloned.1.call-done, bf16[1408,2048]{1,0:T(8,128)(2,1)} %all-gather.11.cloned.1.call-done), kind=kOutput, calls=%fused_computation.31 | convolution fusion | flops 2952790016 | bytes 10747904 | tf_op jit(solution)/shard_map/dot_general | solution.py:31
  300.9 36.5 %all-gather.9.cloned.1.call-done = bf16[1408,2048]{1,0:T(8,128)(2,1)} async-done(((bf16[1408,256]{1,0:T(8,128)(2,1)}), bf16[1408,2048]{1,0:T(8,128)(2,1)}) %all-gather.9.cloned.1.call-update) | async-done | bytes 5767184 | tf_op jit(solution)/shard_map/all_gather | solution.py:27
  337.4 7.4 fusion.9
  344.8 14.8 %all-gather.5.cloned.1.call-done = bf16[512,2048]{1,0:T(8,128)(2,1)} async-done(((bf16[128,2048]{1,0:T(8,128)(2,1)}), bf16[512,2048]{1,0:T(8,128)(2,1)}) %all-gather.5.cloned.1.call-update) | async-done | bytes 2097168 | tf_op jit(solution)/shard_map/all_gather | solution.py:23
  359.6 10.2 %multiply_convert_fusion.4 = (bf16[512,1408]{0,1:T(8,128)(2,1)S(1)}, bf16[512,1408]{0,1:T(8,128)(2,1)}) fusion(f32[512,1408]{0,1:T(8,128)} %fusion.10, f32[512,1408]{0,1:T(8,128)} %fusion.9, bf16[512,2048]{1,0:T(8,128)(2,1)} %all-gather.5.cloned.1.call-done, bf16[1408,4096]{1,0:T(8,128)(2,1)} %constant_dynamic-update-slice_fusion, s32[]{:T(128)S(6)} %select_n.14), kind=kOutput, calls=%fused_computation.9 | convolution fusion | flops 2962161664 | bytes 16515076 | tf_op jit(solution)/shard_map/dot_general | solution.py:33
  369.9 5.0 multiply_convert_fusion.1
  374.9 6.4 multiply_convert_fusion.2
  383.3 7.9 %multiply_convert_fusion = bf16[1408,2048]{1,0:T(8,128)(2,1)} fusion(bf16[512,2048]{1,0:T(8,128)(2,1)S(1)} %copy-done.2, f32[512,1408]{0,1:T(8,128)} %fusion.9, f32[512,1408]{0,1:T(8,128)} %fusion.10), kind=kOutput, calls=%fused_computation | convolution fusion | flops 2962882560 | bytes 13631488 | tf_op jit(solution)/shard_map/dot_general | solution.py:51
  392.6 5.5 fusion.11
  398.0 7.4 add_convert_fusion
  405.4 80.6 %reduce-scatter.9.cloned.1.call-done = bf16[1408,256]{1,0:T(8,128)(2,1)} async-done(((bf16[1408,2048]{1,0:T(8,128)(2,1)}), bf16[1408,256]{1,0:T(8,128)(2,1)}) %reduce-scatter.9.cloned.1.call-update) | async-done | bytes 720912 | tf_op jit(solution)/shard_map/reduce_scatter | solution.py:56
  486.0 2.3 multiply_reduce_fusion.1
  488.4 111.6 %reduce-scatter.7.cloned.1.call-done = bf16[1408,256]{1,0:T(8,128)(2,1)} async-done(((bf16[1408,2048]{1,0:T(8,128)(2,1)}), bf16[1408,256]{1,0:T(8,128)(2,1)}) %reduce-scatter.7.cloned.1.call-update) | async-done | bytes 720912 | tf_op jit(solution)/shard_map/reduce_scatter | solution.py:53
  600.0 2.3 multiply_reduce_fusion.2
  602.3 111.7 %reduce-scatter.11.cloned.1.call-done = bf16[1408,256]{1,0:T(8,128)(2,1)} async-done(((bf16[1408,2048]{1,0:T(8,128)(2,1)}), bf16[1408,256]{1,0:T(8,128)(2,1)}) %reduce-scatter.11.cloned.1.call-update) | async-done | bytes 720912 | tf_op jit(solution)/shard_map/reduce_scatter | solution.py:59
  714.0 2.3 multiply_reduce_fusion
  716.4 35.5 %all-reduce = (f32[1408]{0:T(1024)S(1)}, f32[1408]{0:T(1024)S(1)}, f32[1408]{0:T(1024)S(1)}) all-reduce(f32[1408]{0:T(1024)S(1)} %get-tuple-element.14, f32[1408]{0:T(1024)S(1)} %get-tuple-element.12, f32[1408]{0:T(1024)S(1)} %get-tuple-element.10), channel_id=1, replica_groups=mesh['fs'=8,'tp'=4] {'fs'}, use_global_device_ids=true, to_apply=%region_5.6 | all-reduce | flops 4224 | bytes 33792 | tf_op jit(solution)/shard_map/psum | solution.py:63
  (38 shorter events, 16.1 us)
Async XLA Ops:
  7.2 79.0 %copy-start = (bf16[1408,256]{1,0:T(8,128)(2,1)S(1)}, bf16[1408,256]{1,0:T(8,128)(2,1)}, u32[]{:S(2)}) copy-start(bf16[1408,256]{1,0:T(8,128)(2,1)} %param.8) | copy-start | bytes 2162692
  7.2 285.5 %all-gather.7.cloned.1.call-start = ((), (), s32[]{:S(2)}) async-start(), calls=%async_computation.5 | async-start | bytes 2621440 | tf_op jit(solution)/shard_map/all_gather | solution.py:22
  7.9 284.8 %all-gather.11.cloned.1.call-start = ((), (), s32[]{:S(2)}) async-start(), calls=%async_computation.7 | async-start | bytes 6488064 | tf_op jit(solution)/shard_map/all_gather | solution.py:26
  8.7 328.8 %all-gather.9.cloned.1.call-start = ((), (), s32[]{:S(2)}) async-start(), calls=%async_computation.6 | async-start | bytes 6488064 | tf_op jit(solution)/shard_map/all_gather | solution.py:27
  9.4 350.2 %all-gather.5.cloned.1.call-start = ((), (), s32[]{:S(2)}) async-start(), calls=%async_computation.4 | async-start | bytes 2621440 | tf_op jit(solution)/shard_map/all_gather | solution.py:23
  9.4 21.8 %collective-permute-start = (bf16[1408,256]{1,0:T(8,128)(2,1)}, bf16[1408,256]{1,0:T(8,128)(2,1)S(1)}, u32[]{:S(2)}, u32[]{:S(2)}) collective-permute-start(bf16[1408,256]{1,0:T(8,128)(2,1)} %param.8), channel_id=1, source_target_pairs={{0,28},{4,0},{8,4},{12,8},{16,12},{20,16},{24,20},{28,24},{1,29},{... | collective-permute-start | bytes 2162696 | tf_op jit(solution)/shard_map/ppermute | solution.py:13
  32.5 53.7 %collective-permute-start.1 = (bf16[1408,512]{1,0:T(8,128)(2,1)S(1)}, bf16[1408,512]{1,0:T(8,128)(2,1)S(1)}, u32[]{:S(2)}, u32[]{:S(2)}) collective-permute-start(bf16[1408,512]{1,0:T(8,128)(2,1)S(1)} %pad_maximum_fusion.1), channel_id=1, source_target_pairs={{0,24},{4,28},{8,0},{12,4},{16,8},{20,12},{24,16},{28,20},{1,25},{... | collective-permute-start | bytes 4325384 | tf_op jit(solution)/shard_map/ppermute | solution.py:13
  88.1 193.9 %collective-permute-start.2 = (bf16[1408,1024]{1,0:T(8,128)(2,1)}, bf16[1408,1024]{1,0:T(8,128)(2,1)}, u32[]{:S(2)}, u32[]{:S(2)}) collective-permute-start(bf16[1408,1024]{1,0:T(8,128)(2,1)} %pad_maximum_fusion), channel_id=1, source_target_pairs={{0,16},{4,20},{8,24},{12,28},{16,0},{20,4},{24,8},{28,12},{1,17},{... | collective-permute-start | bytes 8650760 | tf_op jit(solution)/shard_map/ppermute | solution.py:13
  88.2 397.9 %reduce-scatter.9.cloned.1.call-start = ((), (), s32[]{:S(2)}) async-start(), calls=%async_computation.10 | async-start | bytes 6488064 | tf_op jit(solution)/shard_map/reduce_scatter | solution.py:56
  292.7 44.7 %copy-start.1 = (bf16[512,2048]{1,0:T(8,128)(2,1)S(1)}, bf16[512,2048]{1,0:T(8,128)(2,1)}, u32[]{:S(2)}) copy-start(bf16[512,2048]{1,0:T(8,128)(2,1)} %all-gather.7.cloned.1.call-done) | copy-start | bytes 6291460
  374.8 225.1 %reduce-scatter.7.cloned.1.call-start = ((), (), s32[]{:S(2)}) async-start(), calls=%async_computation.9 | async-start | bytes 6488064 | tf_op jit(solution)/shard_map/reduce_scatter | solution.py:53
  381.3 2.0 copy-start.2
  381.3 332.7 %reduce-scatter.11.cloned.1.call-start = ((), (), s32[]{:S(2)}) async-start(), calls=%async_computation.11 | async-start | bytes 6488064 | tf_op jit(solution)/shard_map/reduce_scatter | solution.py:59
  391.2 1.4 copy-start.3
  391.2 361.8 %reduce-scatter.5.cloned.1.call-start = ((), (), s32[]{:S(2)}) async-start(), calls=%async_computation.8 | async-start | bytes 2621440 | tf_op jit(solution)/shard_map/reduce_scatter | solution.py:40
Sparse Core Ops, SparseCore 0:
  9.5 25.2 all-gather.6
  36.9 195.9 all-gather.10
  235.0 102.4 all-gather.8
  338.8 20.7 all-gather.4
  375.0 111.0 reduce-scatter.8
  489.5 110.3 reduce-scatter.6
  603.6 110.3 reduce-scatter.10
  717.1 30.4 reduce-scatter.4
